TPU v7x, 32 devices: a whole 2x2x4 slice. The times are simulated.
32 devices in a mesh: sp: 16 (over z, x, core), tp: 2 (over y).
Axes of the slice: x: 2, y: 2, z: 4, core: 2. Of those that a mesh axis runs over, the one named last changes fastest.
Arguments:
- skip_connection_stream: bfloat16 [12288, 2048], P('sp'), may hold values from -6 to 6
- probing_vectors: bfloat16 [12288, 512], P('sp', 'tp'), may hold values from -6 to 6
- addressing_vectors: bfloat16 [12288, 512], P('sp', 'tp'), may hold values from -6 to 6
- mapped_payloads: bfloat16 [12288, 1024], P('sp', 'tp'), may hold values from -6 to 6
- emission_switch: bfloat16 [12288, 1024], P('sp', 'tp'), may hold values from -6 to 6
- lapse_preactivation: bfloat16 [12288, 512], P('sp', 'tp')
- lapse_shift_entries: float32 [512], P('tp')
- surplus_attenuation_terms: float32 [12288], P('sp'), may hold values from -0.7 to 0
- passage_label_per_token: int32 [12288], P('sp'), may hold values from 0 to 3, never falling along the last dimension, each value on 1 to 6144 neighbouring positions
- attention_group_rescaler: float32 [128], replicated, may hold values from 0.1 to 1.9
- emission_projector: bfloat16 [1024, 2048], P('tp'), may hold values from -0.1875 to 0.1875
- perceptron_rescaler: float32 [2048], replicated, may hold values from 0.1 to 1.9
- switching_projector: bfloat16 [2048, 5632], P('sp', 'tp'), may hold values from -0.125 to 0.125
- widening_projector: bfloat16 [2048, 5632], P('sp', 'tp'), may hold values from -0.125 to 0.125
- shrinking_projector: bfloat16 [5632, 2048], P('tp', 'sp'), may hold values from -0.078125 to 0.078125
Outputs:
- layer_out: bfloat16 [12288, 2048], P(('sp', 'tp'))
Inputs may be any that keep to these rules, and one draw needn't show every extreme that they name: `passage_label_per_token`: document numbers never fall along the sequence; a document holds at most 6144 positions.
All inputs are finite; a program needn't handle non-finite values.
Results may differ from a plain program's by a relative error of at most 0.014.
Values may be sent and summed in bfloat16 or wider, within the bound.
A program may use at most 128 MiB of HBM per device.

v0:
```python
import jax
import jax.numpy as jnp
from jax import lax
from jax.sharding import PartitionSpec as P

DK = 64
DV = 128
BLOCK = 64
eps = 1e-06
sharpness_factor = 16.0


def entering(shard, axis, join, neutral):
    place = lax.axis_index(axis)
    gathered = jax.tree.map(
        lambda a, kind: lax.all_gather(a.astype(kind), axis),
        shard,
        jax.tree.map(lambda a: jnp.bfloat16 if a.dtype == jnp.float32 else a.dtype, shard),
    )
    state = jax.tree.map(lambda a, e: jnp.zeros_like(a) + jnp.asarray(e, a.dtype), shard, neutral)

    def one(turn, state):
        return join(
            state,
            jax.tree.map(
                lambda a, own: lax.dynamic_index_in_dim(a, turn, 0, False).astype(own.dtype),
                gathered,
                shard,
            ),
        )

    return lax.fori_loop(0, place, one, state)


def head_split(array, heads):
    return array.reshape(array.shape[0], heads, -1).transpose(1, 0, 2)


def block_pass(
    query_head_rows,
    key_heads,
    value_heads,
    decay_heads,
    documents,
    recurrent_state,
    last_doc,
    offset,
    span,
):
    heads, length, _ = query_head_rows.shape
    blocks = length // span
    middle = span // 2

    def to_blocks(array):
        return array.reshape(heads, blocks, span, array.shape[-1]).transpose(1, 0, 2, 3)

    lower = jnp.tril(jnp.ones((span, span), dtype=bool))

    def step(carry, inputs):
        recurrent_state, last_doc, offset = carry
        query_block, key_blk, value_block, piece_attenuation, doc_blk = inputs
        cumulative_decay = jnp.cumsum(piece_attenuation, axis=1)
        previous_valid = (doc_blk == last_doc).astype(jnp.float32)
        cross_block_output = (
            jnp.einsum("gfl,glm->gfm", query_block * jnp.exp(cumulative_decay), recurrent_state)
            * previous_valid[None, :, None]
        )
        centre = cumulative_decay[:, middle : middle + 1, :]
        query_scaled = query_block * jnp.exp(cumulative_decay - centre)
        key_scaled = key_blk * jnp.exp(centre - cumulative_decay)
        same = (doc_blk[:, None] == doc_blk[None, :]) & lower
        raw_scores = jnp.einsum("hik,hjk->hij", query_scaled, key_scaled)
        scores = jnp.where(same[None, :, :], raw_scores, 0.0)
        result = cross_block_output + jnp.einsum("hij,hjv->hiv", scores, value_block)
        final_memory_summary = cumulative_decay[:, -1, :]
        last_valid = (doc_blk[-1] == last_doc).astype(jnp.float32)
        tail_ok = (doc_blk == doc_blk[-1]).astype(jnp.float32)
        decayed_keys = (
            key_blk
            * jnp.exp(final_memory_summary[:, None, :] - cumulative_decay)
            * tail_ok[None, :, None]
        )
        recurrent_state = recurrent_state * jnp.exp(final_memory_summary)[
            :, :, None
        ] * last_valid + jnp.einsum("wrz,wrs->wzs", decayed_keys, value_block)
        return (
            (recurrent_state, doc_blk[-1], offset + final_memory_summary),
            (result, cumulative_decay + offset[:, None, :]),
        )

    carry, outputs = lax.scan(
        step,
        (recurrent_state, last_doc, offset),
        (
            to_blocks(query_head_rows),
            to_blocks(key_heads),
            to_blocks(value_heads),
            to_blocks(decay_heads),
            documents.reshape(blocks, span),
        ),
    )
    result, running_state = outputs
    result = result.transpose(1, 0, 2, 3).reshape(heads, length, -1)
    running_state = running_state.transpose(1, 0, 2, 3).reshape(heads, length, -1)
    return (carry[0], carry[2], result, running_state)


def join_spans(earlier, later):
    linked = ((earlier[3] == later[2]) | (earlier[3] < 0.0) | (later[2] < 0.0)).astype(jnp.float32)
    decay_total = earlier[0] * later[0] * linked
    state_total = earlier[1] * (later[0] * linked)[:, :, None] + later[1]
    first_doc = jnp.where(earlier[2] < 0.0, later[2], earlier[2])
    final_doc = jnp.where(later[3] < 0.0, earlier[3], later[3])
    return (decay_total, state_total, first_doc, final_doc)


def rms_rows(rows, gain):
    wide = rows.astype(jnp.float32)
    return (wide * lax.rsqrt(jnp.mean(wide * wide, axis=-1, keepdims=True) + eps) * gain).astype(
        jnp.bfloat16
    )


def per_device(
    skip_connection_stream,
    probing_vectors,
    addressing_vectors,
    mapped_payloads,
    emission_switch,
    lapse_preactivation,
    lapse_shift_entries,
    surplus_attenuation_terms,
    passage_label_per_token,
    attention_group_rescaler,
    emission_projector,
    perceptron_rescaler,
    switching_projector,
    widening_projector,
    shrinking_projector,
):
    rows_here = skip_connection_stream.shape[0]
    heads_here = probing_vectors.shape[1] // DK
    keeping_exponent = (
        jax.nn.log_sigmoid(lapse_preactivation.astype(jnp.float32) + lapse_shift_entries[None, :])
        / sharpness_factor
        + surplus_attenuation_terms[:, None]
    )
    query_head_rows = head_split(probing_vectors.astype(jnp.float32) * DK ** (-0.5), heads_here)
    key_heads = head_split(addressing_vectors.astype(jnp.float32), heads_here)
    value_heads = head_split(mapped_payloads.astype(jnp.float32), heads_here)
    decay_heads = head_split(keeping_exponent, heads_here)
    zero_state = jnp.zeros((heads_here, DK, DV), jnp.float32)
    state_local, total_log, local_out, running_state = block_pass(
        query_head_rows,
        key_heads,
        value_heads,
        decay_heads,
        passage_label_per_token,
        zero_state,
        passage_label_per_token[0],
        jnp.zeros((heads_here, DK), jnp.float32),
        BLOCK,
    )
    unbroken = (passage_label_per_token[0] == passage_label_per_token[-1]).astype(jnp.float32)
    summary = (
        jnp.exp(total_log) * unbroken,
        state_local,
        passage_label_per_token[0].astype(jnp.float32),
        passage_label_per_token[-1].astype(jnp.float32),
    )
    identity = (
        jnp.ones_like(total_log),
        jnp.zeros_like(state_local),
        jnp.full((), -1.0, jnp.float32),
        jnp.full((), -1.0, jnp.float32),
    )
    carried_state = entering(summary, "sp", join_spans, identity)
    reaches = (passage_label_per_token.astype(jnp.float32) == carried_state[3]).astype(jnp.float32)
    incoming = (
        jnp.einsum("qlj,qjf->qlf", query_head_rows * jnp.exp(running_state), carried_state[1])
        * reaches[None, :, None]
    )
    attn = local_out + incoming
    normed_attn = (
        attn
        * lax.rsqrt(jnp.mean(attn * attn, axis=-1, keepdims=True) + eps)
        * attention_group_rescaler
    )
    flat = normed_attn.transpose(1, 0, 2).reshape(rows_here, heads_here * DV)
    gated = (flat * jax.nn.silu(emission_switch.astype(jnp.float32))).astype(jnp.bfloat16)
    share_rows = rows_here // lax.axis_size("tp")
    own_start = lax.axis_index("tp") * share_rows
    mixed = lax.psum(
        jnp.dot(gated, emission_projector, preferred_element_type=jnp.float32).astype(jnp.bfloat16),
        "tp",
    ).astype(jnp.float32)
    first_all = (skip_connection_stream.astype(jnp.float32) + mixed).astype(jnp.bfloat16)
    normed = rms_rows(first_all, perceptron_rescaler)
    first_own = lax.dynamic_slice_in_dim(first_all, own_start, share_rows, 0)
    gate = jnp.dot(
        normed,
        lax.all_gather(switching_projector, "sp", axis=0, tiled=True),
        preferred_element_type=jnp.float32,
    )
    upper = jnp.dot(
        normed,
        lax.all_gather(widening_projector, "sp", axis=0, tiled=True),
        preferred_element_type=jnp.float32,
    )
    hidden = (jax.nn.silu(gate) * upper).astype(jnp.bfloat16)
    terms = jnp.dot(
        hidden,
        lax.all_gather(shrinking_projector, "sp", axis=1, tiled=True),
        preferred_element_type=jnp.float32,
    )
    ffn_out = lax.psum_scatter(
        terms.astype(jnp.bfloat16), "tp", scatter_dimension=0, tiled=True
    ).astype(jnp.float32)
    return (first_own.astype(jnp.float32) + 0.5 * ffn_out).astype(jnp.bfloat16)


def solution(mesh):
    placed = (
        P("sp", None),
        P("sp", "tp"),
        P("sp", "tp"),
        P("sp", "tp"),
        P("sp", "tp"),
        P("sp", "tp"),
        P("tp"),
        P("sp"),
        P("sp"),
        P(),
        P("tp", None),
        P(),
        P("sp", "tp"),
        P("sp", "tp"),
        P("tp", "sp"),
    )
    return jax.shard_map(
        per_device, mesh=mesh, in_specs=placed, out_specs=P(("sp", "tp"), None), check_vma=False
    )
```

profile of v0, /device:TPU:0, one launch (start us, length us, event | category | flops | bytes accessed | tf_op | source)
XLA Modules:
  0.0 747.7 jit_solution(6886762841094768849)
XLA Ops:
  6.5 1.5 fusion.63
  10.6 1.8 reshape.144
  14.6 2.7 reshape.150
  19.1 1.8 reshape.137
  21.0 1.4 copy.49
  23.6 117.2 %while.35 = (s32[]{:T(128)}, f32[4,64,128]{2,1,0:T(8,128)S(1)}, s32[]{:T(128)}, f32[4,64]{1,0:T(4,128)S(1)}, f32[12,4,64,128]{3,2,0,1:T(8,128)}, /*index=5*/f32[...) while((s32[]{:T(128)}, f32[4,64,128]{2,1,0:T(8,128)S(1)}, ...), condition=%wide.region_2.3_spmd.clone, body=%wide.region_0.2_spmd.clone.sunk | while | flops 16118533 | bytes 2851019 | solution.py:91
  25.2 1.7 constant_dynamic-slice_fusion.7
  27.4 1.8 fusion.85
  34.9 1.7 constant_dynamic-slice_fusion.7
  37.2 1.8 fusion.85
  44.7 1.7 constant_dynamic-slice_fusion.7
  46.9 1.8 fusion.85
  54.5 1.7 constant_dynamic-slice_fusion.7
  56.7 1.8 fusion.85
  64.3 1.7 constant_dynamic-slice_fusion.7
  66.5 1.8 fusion.85
  74.0 1.7 constant_dynamic-slice_fusion.7
  76.2 1.8 fusion.85
  83.8 1.7 constant_dynamic-slice_fusion.7
  86.0 1.8 fusion.85
  93.6 1.7 constant_dynamic-slice_fusion.7
  95.8 1.8 fusion.85
  103.3 1.7 constant_dynamic-slice_fusion.7
  105.5 1.8 fusion.85
  113.1 1.7 constant_dynamic-slice_fusion.7
  115.3 1.8 fusion.85
  122.8 1.7 constant_dynamic-slice_fusion.7
  125.1 1.8 fusion.85
  132.6 1.7 constant_dynamic-slice_fusion.7
  134.8 1.8 fusion.85
  144.9 35.1 %all-reduce.2 = (bf16[16]{0:T(256)(128)(2,1)S(1)}, bf16[16]{0:T(256)(128)(2,1)S(1)}) all-reduce(bf16[16]{0:T(256)(128)(2,1)S(1)} %dynamic-update-slice, bf16[16]{0:T(256)(128)(2,1)S(1)} %dynamic-update-slice.1), channel_id=1, replica_groups=mesh['sp'=16,'tp'=2] {'sp'}, use_global_device_ids=true, to_apply=%add | all-reduce | flops 32 | bytes 128
  181.2 2.8 exponential_bitcast_fusion
  184.0 3.0 copy.57
  186.9 2.7 exp.47
  189.6 3.1 copy.58
  192.8 17.1 %all-gather.2 = bf16[16,4,64]{2,1,0:T(4,128)(2,1)S(1)} all-gather(bf16[1,4,64]{2,1,0:T(4,128)(2,1)S(1)} %fusion.58), channel_id=2, replica_groups=mesh['sp'=16,'tp'=2] {'sp'}, dimensions={0}, use_global_device_ids=true | all-gather | bytes 8704 | tf_op jit(solution)/shard_map/all_gather | solution.py:16
  210.0 2.1 multiply_reduce_fusion
  213.5 3.0 copy.59
  216.6 4.9 convolution_convert_fusion
  223.6 154.7 %all-reduce.5.cloned.1.call-done = bf16[768,2048]{1,0:T(8,128)(2,1)} async-done(((bf16[768,2048]{1,0:T(8,128)(2,1)}), bf16[768,2048]{1,0:T(8,128)(2,1)}) %all-reduce.5.cloned.1.call-update) | async-done | bytes 3145744 | tf_op jit(solution)/shard_map/psum | solution.py:193
  378.3 6.0 fusion.36
  384.3 90.3 %all-gather.8.cloned.1.call-done = bf16[2048,2816]{1,0:T(8,128)(2,1)} async-done(((bf16[128,2816]{1,0:T(8,128)(2,1)}), bf16[2048,2816]{1,0:T(8,128)(2,1)}) %all-gather.8.cloned.1.call-update) | async-done | bytes 11534352 | tf_op jit(solution)/shard_map/all_gather | solution.py:202
  474.6 15.9 %fusion.49 = f32[768,2816]{1,0:T(8,128)} fusion(bf16[2048,2816]{1,0:T(8,128)(2,1)} %all-gather.8.cloned.1.call-done, bf16[768,2048]{1,0:T(8,128)(2,1)} %get-tuple-element.262, f32[2048]{0:T(1024)S(1)} %copy-done.9, f32[768]{0:T(1024)S(1)} %add_rsqrt_fusion.1), kind=kOutput, calls=%fused_computation.73 | convolution fusion | flops 8864661504 | bytes 23342080 | tf_op jit(solution)/shard_map/dot_general | solution.py:200
  490.6 78.5 %all-gather.10.cloned.1.call-done = bf16[2048,2816]{1,0:T(8,128)(2,1)} async-done(((bf16[128,2816]{1,0:T(8,128)(2,1)}), bf16[2048,2816]{1,0:T(8,128)(2,1)}) %all-gather.10.cloned.1.call-update) | async-done | bytes 11534352 | tf_op jit(solution)/shard_map/all_gather | solution.py:207
  569.0 97.2 %all-gather.12.cloned.1.call-done = bf16[2816,2048]{1,0:T(8,128)(2,1)} async-done(((bf16[2816,128]{1,0:T(8,128)(2,1)}), bf16[2816,2048]{1,0:T(8,128)(2,1)}) %all-gather.12.cloned.1.call-update) | async-done | bytes 11534352 | tf_op jit(solution)/shard_map/all_gather | solution.py:213
  666.2 29.2 %fusion.41 = bf16[768,2048]{1,0:T(8,128)(2,1)} fusion(bf16[2816,2048]{1,0:T(8,128)(2,1)} %all-gather.12.cloned.1.call-done, f32[768,2816]{1,0:T(8,128)} %fusion.49, bf16[2048,2816]{1,0:T(8,128)(2,1)} %all-gather.10.cloned.1.call-done, bf16[768,2048]{1,0:T(8,128)(2,1)} %get-tuple-element.262, f32[2048]{0:T(1024)S(1)} %copy-done.9, f32[768]{0:T(1024)S(1)} %add_rsqrt_fusion.1), kind=kOutput, calls=%fused_computation.57 | convolution fusion | flops 17737580544 | bytes 38022144 | tf_op jit(solution)/shard_map/dot_general | solution.py:211
  695.4 41.7 %reduce-scatter.2.cloned.1.call-done = bf16[384,2048]{1,0:T(8,128)(2,1)} async-done(((bf16[768,2048]{1,0:T(8,128)(2,1)}), bf16[384,2048]{1,0:T(8,128)(2,1)}) %reduce-scatter.2.cloned.1.call-update) | async-done | bytes 1572880 | tf_op jit(solution)/shard_map/reduce_scatter | solution.py:216
  737.1 3.7 add_convert_fusion.1
  (228 shorter events, 73.2 us)
Async XLA Ops:
  6.5 210.0 %copy-start = (bf16[512,2048]{1,0:T(8,128)(2,1)S(1)}, bf16[512,2048]{1,0:T(8,128)(2,1)}, u32[]{:S(2)}) copy-start(bf16[512,2048]{1,0:T(8,128)(2,1)} %param.29) | copy-start | bytes 6291460
  6.5 203.4 %all-gather.14.cloned.1.call-start = ((), (), s32[]{:S(2)}) async-start(), calls=%async_computation.6 | async-start | bytes 1114112 | tf_op jit(solution)/shard_map/all_gather | solution.py:16
  10.6 6.7 copy-start.2
  12.4 6.1 copy-start.5
  12.5 6.1 copy-start.6
  23.6 119.2 %copy-start.10 = (u32[32]{0:T(128)S(1)}, u32[32]{0:T(128)}, u32[]{:S(2)}) copy-start(u32[32]{0:T(128)} %constant.98) | copy-start | bytes 388
  141.5 236.9 %all-reduce.5.cloned.1.call-start = ((), (), s32[]{:S(2)}) async-start(), calls=%async_computation.1 | async-start | bytes 6291456 | tf_op jit(solution)/shard_map/psum | solution.py:193
  189.6 20.3 %copy-start.4 = (s32[768]{0:T(1024)S(1)}, s32[768]{0:T(1024)}, u32[]{:S(2)}) copy-start(s32[768]{0:T(1024)} %param.27) | copy-start | bytes 9220
  189.6 20.4 %copy-start.3 = (f32[768,256]{0,1:T(8,128)S(1)}, f32[768,256]{0,1:T(8,128)}, u32[]{:S(2)}) copy-start(f32[768,256]{0,1:T(8,128)} %copy-done.2) | copy-start | bytes 2359300
  209.9 2.2 copy-start.7
  212.2 4.4 copy-start.8
  221.5 253.2 %all-gather.8.cloned.1.call-start = ((), (), s32[]{:S(2)}) async-start(), calls=%async_computation.2 | async-start | bytes 12255232 | tf_op jit(solution)/shard_map/all_gather | solution.py:202
  222.2 346.8 %all-gather.10.cloned.1.call-start = ((), (), s32[]{:S(2)}) async-start(), calls=%async_computation.3 | async-start | bytes 12255232 | tf_op jit(solution)/shard_map/all_gather | solution.py:207
  222.8 443.4 %all-gather.12.cloned.1.call-start = ((), (), s32[]{:S(2)}) async-start(), calls=%async_computation.4 | async-start | bytes 12255232 | tf_op jit(solution)/shard_map/all_gather | solution.py:213
  223.4 251.3 %copy-start.9 = (f32[2048]{0:T(1024)S(1)}, f32[2048]{0:T(1024)}, u32[]{:S(2)}) copy-start(f32[2048]{0:T(1024)} %param.30) | copy-start | bytes 24580
  223.4 513.7 %reduce-scatter.2.cloned.1.call-start = ((), (), s32[]{:S(2)}) async-start(), calls=%async_computation.5 | async-start | bytes 4718592 | tf_op jit(solution)/shard_map/reduce_scatter | solution.py:216
  695.4 45.4 %copy-start.1 = (bf16[512,2048]{1,0:T(8,128)(2,1)S(1)}, bf16[512,2048]{1,0:T(8,128)(2,1)}, u32[]{:S(2)}) copy-start(bf16[512,2048]{1,0:T(8,128)(2,1)} %param.29) | copy-start | bytes 6291460
Sparse Core Ops, SparseCore 0:
  141.6 40.5 all-gather.13
  221.6 156.6 all-reduce.4
  380.6 93.9 all-gather.7
  476.8 92.2 all-gather.9
  571.0 95.1 all-gather.11
  695.5 41.5 reduce-scatter.1
where the time goes:
time: 752 us; the launch traced here: 748 us
  waiting for transfers between devices  464 us (62%)
  matrix products  89.2 us (12%)
  local copies, waits for them, and re-layouts  78.8 us (10%)
  blocking collectives  52.2 us (7%)
  other arithmetic  31.1 us (4%)
  between operations  16.8 us (2%)
  loops' own time  15 us (2%)
    psum x1, waiting for transfers between devices, per_device(): lax.psum(jnp.dot(gated, emission_projector, preferred_element_type=jnp.fl...  155 us
    all_gather x1, waiting for transfers between devices, per_device(): lax.all_gather(shrinking_projector, 'sp', axis=1, tiled=True)  97.2 us
    all_gather x1, waiting for transfers between devices, per_device(): lax.all_gather(switching_projector, 'sp', axis=0, tiled=True)  90.3 us
    all_gather x1, waiting for transfers between devices, per_device(): lax.all_gather(widening_projector, 'sp', axis=0, tiled=True)  78.5 us
    reduce_scatter x1, waiting for transfers between devices, per_device(): lax.psum_scatter(terms.astype(jnp.bfloat16), 'tp', scatter_dimension=0, t...  41.7 us
    dynamic_slice x60, local copies, waits for them, and re-layouts, block_pass(): lax.scan(step, (recurrent_state, last_doc, offset), (to_blocks(query_head...  40.2 us
    unnamed x1, blocking collectives  35.1 us
    dot_general x1, matrix products, per_device(): jnp.dot(hidden, lax.all_gather(shrinking_projector, 'sp', axis=1, tiled=T...  29.2 us
  transfers between devices with their start and end apart: 6, of which 5 were waited for; matrix products, arithmetic and copies ran while one was open for 5% of the time, Pallas kernels for 0%

commit v1 on v0

--- a/solution.py
+++ b/solution.py
@@ -210,7 +210,7 @@
     hidden = (jax.nn.silu(gate) * upper).astype(jnp.bfloat16)
     terms = jnp.dot(
         hidden,
-        lax.all_gather(shrinking_projector, "sp", axis=1, tiled=True),
+        jnp.concatenate(lax.all_gather(shrinking_projector, "sp"), axis=1),
         preferred_element_type=jnp.float32,
     )
     ffn_out = lax.psum_scatter(

time: 752 us -> 754 us (level)
  waiting for transfers between devices: 464 us -> 446 us
  local copies, waits for them, and re-layouts: 78.8 us -> 94 us
    reshape x0 -> x1, local copies, waits for them, and re-layouts: none -> 15.2 us  [per_device(): jnp.concatenate(lax.all_gather(shrinking_projector, 'sp'), axis=1)]
    all_gather x1, waiting for transfers between devices: 90.3 us -> 79.2 us  [per_device(): lax.all_gather(switching_projector, 'sp', axis=0, tiled=True)]
  transfers between devices with their start and end apart: 6 -> 6, of which waited for: 5 -> 5; matrix products, arithmetic and copies ran while one was open for 5% -> 7% of each run, Pallas kernels for 0% -> 0%
where the time goes in v1:
time: 754 us; the launch traced here: 750 us
  waiting for transfers between devices  446 us (59%)
  matrix products  94.1 us (12%)
  local copies, waits for them, and re-layouts  94 us (12%)
  blocking collectives  52.2 us (7%)
  other arithmetic  31.1 us (4%)
  between operations  16.8 us (2%)
  loops' own time  15 us (2%)
    psum x1, waiting for transfers between devices, per_device(): lax.psum(jnp.dot(gated, emission_projector, preferred_element_type=jnp.fl...  155 us
    all_gather x1, waiting for transfers between devices, per_device(): lax.all_gather(shrinking_projector, 'sp')  90.3 us
    all_gather x1, waiting for transfers between devices, per_device(): lax.all_gather(switching_projector, 'sp', axis=0, tiled=True)  79.2 us
    all_gather x1, waiting for transfers between devices, per_device(): lax.all_gather(widening_projector, 'sp', axis=0, tiled=True)  78.6 us
    reduce_scatter x1, waiting for transfers between devices, per_device(): lax.psum_scatter(terms.astype(jnp.bfloat16), 'tp', scatter_dimension=0, t...  41.8 us
    dynamic_slice x60, local copies, waits for them, and re-layouts, block_pass(): lax.scan(step, (recurrent_state, last_doc, offset), (to_blocks(query_head...  40.2 us
    unnamed x1, blocking collectives  35.1 us
    dot_general x1, matrix products, per_device(): jnp.dot(hidden, jnp.concatenate(lax.all_gather(shrinking_projector, 'sp')...  34.2 us
  transfers between devices with their start and end apart: 6, of which 5 were waited for; matrix products, arithmetic and copies ran while one was open for 7% of the time, Pallas kernels for 0%

profile of v1, /device:TPU:0, one launch (start us, length us, event | category | flops | bytes accessed | tf_op | source)
XLA Modules:
  0.0 750.0 jit_solution(3865380202980922380)
XLA Ops:
  6.5 1.5 fusion.60
  10.6 1.8 reshape.150
  14.6 2.7 reshape.158
  19.1 1.8 reshape.143
  23.6 117.2 %while.35 = (s32[]{:T(128)}, f32[4,64,128]{2,1,0:T(8,128)S(1)}, s32[]{:T(128)}, f32[4,64]{1,0:T(4,128)S(1)}, f32[12,4,64,128]{3,2,0,1:T(8,128)}, /*index=5*/f32[...) while((s32[]{:T(128)}, f32[4,64,128]{2,1,0:T(8,128)S(1)}, ...), condition=%wide.region_2.3_spmd.clone, body=%wide.region_0.2_spmd.clone.sunk | while | flops 16118533 | bytes 2851019 | solution.py:91
  25.2 1.7 constant_dynamic-slice_fusion.7
  27.4 1.8 fusion.82
  34.9 1.7 constant_dynamic-slice_fusion.7
  37.2 1.8 fusion.82
  44.7 1.7 constant_dynamic-slice_fusion.7
  46.9 1.8 fusion.82
  54.5 1.7 constant_dynamic-slice_fusion.7
  56.7 1.8 fusion.82
  64.3 1.7 constant_dynamic-slice_fusion.7
  66.5 1.8 fusion.82
  74.0 1.7 constant_dynamic-slice_fusion.7
  76.2 1.8 fusion.82
  83.8 1.7 constant_dynamic-slice_fusion.7
  86.0 1.8 fusion.82
  93.6 1.7 constant_dynamic-slice_fusion.7
  95.8 1.8 fusion.82
  103.3 1.7 constant_dynamic-slice_fusion.7
  105.5 1.8 fusion.82
  113.1 1.7 constant_dynamic-slice_fusion.7
  115.3 1.8 fusion.82
  122.8 1.7 constant_dynamic-slice_fusion.7
  125.1 1.8 fusion.82
  132.6 1.7 constant_dynamic-slice_fusion.7
  134.8 1.8 fusion.82
  144.9 35.1 %all-reduce.2 = (bf16[16]{0:T(256)(128)(2,1)S(1)}, bf16[16]{0:T(256)(128)(2,1)S(1)}) all-reduce(bf16[16]{0:T(256)(128)(2,1)S(1)} %dynamic-update-slice, bf16[16]{0:T(256)(128)(2,1)S(1)} %dynamic-update-slice.1), channel_id=1, replica_groups=mesh['sp'=16,'tp'=2] {'sp'}, use_global_device_ids=true, to_apply=%add | all-reduce | flops 32 | bytes 128
  181.2 2.8 exponential_bitcast_fusion
  184.0 3.0 copy.58
  186.9 2.7 exp.47
  189.6 3.1 copy.59
  192.8 17.1 %all-gather.3 = bf16[16,4,64]{2,1,0:T(4,128)(2,1)S(1)} all-gather(bf16[1,4,64]{2,1,0:T(4,128)(2,1)S(1)} %fusion.55), channel_id=2, replica_groups=mesh['sp'=16,'tp'=2] {'sp'}, dimensions={0}, use_global_device_ids=true | all-gather | bytes 8704 | tf_op jit(solution)/shard_map/all_gather | solution.py:16
  210.0 2.1 multiply_reduce_fusion
  213.5 3.0 copy.60
  216.6 4.9 convolution_convert_fusion
  223.6 154.7 %all-reduce.5.cloned.1.call-done = bf16[768,2048]{1,0:T(8,128)(2,1)} async-done(((bf16[768,2048]{1,0:T(8,128)(2,1)}), bf16[768,2048]{1,0:T(8,128)(2,1)}) %all-reduce.5.cloned.1.call-update) | async-done | bytes 3145744 | tf_op jit(solution)/shard_map/psum | solution.py:193
  378.3 6.0 fusion.36
  384.3 90.3 %all-gather.15.cloned.1.call-done = bf16[45056,128]{1,0:T(8,128)(2,1)} async-done(((bf16[2816,128]{1,0:T(8,128)(2,1)}), bf16[45056,128]{1,0:T(8,128)(2,1)}) %all-gather.15.cloned.1.call-update) | async-done | bytes 11534352 | tf_op jit(solution)/shard_map/all_gather | solution.py:213
  474.6 15.2 %copy.61 = bf16[2816,16,128]{0,2,1:T(8,128)(2,1)} copy(bf16[2816,16,128]{2,0,1:T(8,128)(2,1)} %bitcast.140) | data formatting | bytes 23068672 | tf_op jit(solution)/shard_map/reshape | solution.py:213
  489.9 79.2 %all-gather.9.cloned.1.call-done = bf16[2048,2816]{1,0:T(8,128)(2,1)} async-done(((bf16[128,2816]{1,0:T(8,128)(2,1)}), bf16[2048,2816]{1,0:T(8,128)(2,1)}) %all-gather.9.cloned.1.call-update) | async-done | bytes 11534352 | tf_op jit(solution)/shard_map/all_gather | solution.py:202
  569.0 15.8 %fusion.46 = f32[768,2816]{1,0:T(8,128)} fusion(bf16[2048,2816]{1,0:T(8,128)(2,1)} %all-gather.9.cloned.1.call-done, bf16[768,2048]{1,0:T(8,128)(2,1)} %get-tuple-element.262, f32[2048]{0:T(1024)S(1)} %copy-done.9, f32[768]{0:T(1024)S(1)} %add_rsqrt_fusion.1), kind=kOutput, calls=%fused_computation.71 | convolution fusion | flops 8864661504 | bytes 23342080 | tf_op jit(solution)/shard_map/dot_general | solution.py:200
  584.9 78.6 %all-gather.11.cloned.1.call-done = bf16[2048,2816]{1,0:T(8,128)(2,1)} async-done(((bf16[128,2816]{1,0:T(8,128)(2,1)}), bf16[2048,2816]{1,0:T(8,128)(2,1)}) %all-gather.11.cloned.1.call-update) | async-done | bytes 11534352 | tf_op jit(solution)/shard_map/all_gather | solution.py:207
  663.4 34.2 %convolution_convert_fusion.1 = bf16[768,2048]{1,0:T(8,128)(2,1)} fusion(bf16[2816,2048]{0,1:T(8,128)(2,1)} %bitcast.141, f32[768,2816]{1,0:T(8,128)} %fusion.46, bf16[2048,2816]{1,0:T(8,128)(2,1)} %all-gather.11.cloned.1.call-done, bf16[768,2048]{1,0:T(8,128)(2,1)} %get-tuple-element.262, f32[2048]{0:T(1024)S(1)} %copy-done.9, f32[768]{0:T(1024)S(1)} %add_rsqrt_fusion.1), kind=kOutput, calls=%fused_computation.56 | convolution fusion | flops 17737580544 | bytes 38022144 | tf_op jit(solution)/shard_map/dot_general | solution.py:211
  697.6 41.8 %reduce-scatter.2.cloned.1.call-done = bf16[384,2048]{1,0:T(8,128)(2,1)} async-done(((bf16[768,2048]{1,0:T(8,128)(2,1)}), bf16[384,2048]{1,0:T(8,128)(2,1)}) %reduce-scatter.2.cloned.1.call-update) | async-done | bytes 1572880 | tf_op jit(solution)/shard_map/reduce_scatter | solution.py:216
  739.5 3.7 add_convert_fusion.1
  (229 shorter events, 74.6 us)
Async XLA Ops:
  6.5 210.0 %copy-start = (bf16[512,2048]{1,0:T(8,128)(2,1)S(1)}, bf16[512,2048]{1,0:T(8,128)(2,1)}, u32[]{:S(2)}) copy-start(bf16[512,2048]{1,0:T(8,128)(2,1)} %param.29) | copy-start | bytes 6291460
  6.5 203.4 %all-gather.13.cloned.1.call-start = ((), (), s32[]{:S(2)}) async-start(), calls=%async_computation.5 | async-start | bytes 1114112 | tf_op jit(solution)/shard_map/all_gather | solution.py:16
  10.6 6.7 copy-start.2
  12.4 6.1 copy-start.5
  12.5 6.1 copy-start.6
  23.6 119.2 %copy-start.10 = (u32[32]{0:T(128)S(1)}, u32[32]{0:T(128)}, u32[]{:S(2)}) copy-start(u32[32]{0:T(128)} %constant.98) | copy-start | bytes 388
  141.5 236.9 %all-reduce.5.cloned.1.call-start = ((), (), s32[]{:S(2)}) async-start(), calls=%async_computation.1 | async-start | bytes 6291456 | tf_op jit(solution)/shard_map/psum | solution.py:193
  189.6 20.3 %copy-start.4 = (s32[768]{0:T(1024)S(1)}, s32[768]{0:T(1024)}, u32[]{:S(2)}) copy-start(s32[768]{0:T(1024)} %param.27) | copy-start | bytes 9220
  189.6 20.4 %copy-start.3 = (f32[768,256]{0,1:T(8,128)S(1)}, f32[768,256]{0,1:T(8,128)}, u32[]{:S(2)}) copy-start(f32[768,256]{0,1:T(8,128)} %copy-done.2) | copy-start | bytes 2359300
  209.9 2.2 copy-start.7
  212.2 4.4 copy-start.8
  221.5 253.2 %all-gather.15.cloned.1.call-start = ((), (), s32[]{:S(2)}) async-start(), calls=%async_computation.6 | async-start | bytes 12255232 | tf_op jit(solution)/shard_map/all_gather | solution.py:213
  222.2 346.8 %all-gather.9.cloned.1.call-start = ((), (), s32[]{:S(2)}) async-start(), calls=%async_computation.2 | async-start | bytes 12255232 | tf_op jit(solution)/shard_map/all_gather | solution.py:202
  222.8 440.6 %all-gather.11.cloned.1.call-start = ((), (), s32[]{:S(2)}) async-start(), calls=%async_computation.3 | async-start | bytes 12255232 | tf_op jit(solution)/shard_map/all_gather | solution.py:207
  223.4 516.1 %reduce-scatter.2.cloned.1.call-start = ((), (), s32[]{:S(2)}) async-start(), calls=%async_computation.4 | async-start | bytes 4718592 | tf_op jit(solution)/shard_map/reduce_scatter | solution.py:216
  474.6 94.4 %copy-start.9 = (f32[2048]{0:T(1024)S(1)}, f32[2048]{0:T(1024)}, u32[]{:S(2)}) copy-start(f32[2048]{0:T(1024)} %param.30) | copy-start | bytes 24580
  697.6 45.5 %copy-start.1 = (bf16[512,2048]{1,0:T(8,128)(2,1)S(1)}, bf16[512,2048]{1,0:T(8,128)(2,1)}, u32[]{:S(2)}) copy-start(bf16[512,2048]{1,0:T(8,128)(2,1)} %param.29) | copy-start | bytes 6291460
Sparse Core Ops, SparseCore 0:
  141.6 40.5 all-gather.12
  221.6 156.6 all-reduce.4
  380.6 93.9 all-gather.14
  476.8 92.2 all-gather.8
  571.2 92.2 all-gather.10
  697.7 41.6 reduce-scatter.1
